TPU v7x, 32 devices: a whole 2x2x4 slice. The times are simulated.
32 devices in a mesh: fs: 8 (over z, y), tp: 4 (over x, core).
Axes of the slice: x: 2, y: 2, z: 4, core: 2. Of those that a mesh axis runs over, the one named last changes fastest.
Arguments:
- saved_inputs: bfloat16 [16384, 4096], P('fs'), may hold values from -6 to 6
- value_cot: bfloat16 [16384, 1024], P('fs', 'tp'), may hold values from -6 to 6
- gate_cot: bfloat16 [16384, 1024], P('fs', 'tp'), may hold values from -6 to 6
- point_inputs: bfloat16 [16384, 1024], P('fs'), may hold values from -6 to 6
- point_cot: bfloat16 [16384, 1024], P('fs', 'tp'), may hold values from -6 to 6
- master_value: float32 [4096, 1024], P('fs', 'tp'), may hold values from -6 to 6
- master_gate: float32 [4096, 1024], P('fs', 'tp'), may hold values from -6 to 6
- master_point: float32 [1024, 1024], P('fs', 'tp'), may hold values from -6 to 6
- factor_value: bfloat16 [4096, 256], P('fs'), may hold values from -160 to 160
- factor_gate: bfloat16 [4096, 256], P('fs'), may hold values from -160 to 160
- factor_point: bfloat16 [1024, 256], P('fs'), may hold values from -160 to 160
- first_value: float32 [256, 1024], P('fs', 'tp'), may hold values from -6 to 6
- first_gate: float32 [256, 1024], P('fs', 'tp'), may hold values from -6 to 6
- first_point: float32 [256, 1024], P('fs', 'tp'), may hold values from -6 to 6
- second_value: float32 [256, 1024], P('fs', 'tp'), may hold values from 0.2 to 2
- second_gate: float32 [256, 1024], P('fs', 'tp'), may hold values from 0.2 to 2
- second_point: float32 [256, 1024], P('fs', 'tp'), may hold values from 0.2 to 2
Outputs:
- new_value: float32 [4096, 1024], P('fs', 'tp')
- new_gate: float32 [4096, 1024], P('fs', 'tp')
- new_point: float32 [1024, 1024], P('fs', 'tp')
- copy_value: bfloat16 [4096, 1024], P(None, 'tp')
- copy_gate: bfloat16 [4096, 1024], P(None, 'tp')
- copy_point: bfloat16 [1024, 1024], P(None, 'tp')
- next_first_value: float32 [256, 1024], P('fs', 'tp')
- next_first_gate: float32 [256, 1024], P('fs', 'tp')
- next_first_point: float32 [256, 1024], P('fs', 'tp')
- next_second_value: float32 [256, 1024], P('fs', 'tp')
- next_second_gate: float32 [256, 1024], P('fs', 'tp')
- next_second_point: float32 [256, 1024], P('fs', 'tp')
All inputs are finite; a program needn't handle non-finite values.
Results may differ from a plain program's by a relative error of at most 0.0055.
Values may be sent and summed in bfloat16 or wider, within the bound.
A program may use at most 128 MiB of HBM per device.

v0:
```python
import jax
import jax.numpy as jnp
from jax import lax
from jax.sharding import PartitionSpec as P


def contract_rows(left, right):
    return lax.dot_general(
        left, right, (((0,), (0,)), ((), ())), preferred_element_type=jnp.float32
    )


def contract_split(projected, cot):
    upper = projected.astype(jnp.bfloat16)
    lower = (projected - upper.astype(jnp.float32)).astype(jnp.bfloat16)
    return contract_rows(upper, cot) + contract_rows(lower, cot)


def moments(low, first_old, second_old):
    first = 0.8 * first_old + 0.2 * low
    second = 0.9 * second_old + 0.1 * low * low
    return (first, second, first / (jnp.sqrt(second) + 1e-08))


def local(
    saved_inputs,
    value_cot,
    gate_cot,
    point_inputs,
    point_cot,
    master_value,
    master_gate,
    master_point,
    factor_value,
    factor_gate,
    factor_point,
    first_value,
    first_gate,
    first_point,
    second_value,
    second_gate,
    second_point,
):
    total = saved_inputs.shape[0] * lax.axis_size("fs")
    columns = saved_inputs
    proj_value = jnp.dot(
        columns,
        lax.all_gather(factor_value, "fs", axis=0, tiled=True),
        preferred_element_type=jnp.float32,
    )
    proj_gate = jnp.dot(
        columns,
        lax.all_gather(factor_gate, "fs", axis=0, tiled=True),
        preferred_element_type=jnp.float32,
    )
    columns = point_inputs
    proj_point = jnp.dot(
        columns,
        lax.all_gather(factor_point, "fs", axis=0, tiled=True),
        preferred_element_type=jnp.float32,
    )
    low_value = contract_split(proj_value, value_cot)
    low_gate = contract_split(proj_gate, gate_cot)
    low_point = contract_split(proj_point, point_cot)
    summed = (
        lax.psum_scatter(low_value, "fs", scatter_dimension=0, tiled=True),
        lax.psum_scatter(low_gate, "fs", scatter_dimension=0, tiled=True),
        lax.psum_scatter(low_point, "fs", scatter_dimension=0, tiled=True),
    )
    fv, sv, dv = moments(summed[0] / total, first_value, second_value)
    fg, sg, dg = moments(summed[1] / total, first_gate, second_gate)
    fpt, spt, dpt = moments(summed[2] / total, first_point, second_point)
    whole_v, whole_g, whole_p = (
        lax.all_gather(dv, "fs", axis=0, tiled=True),
        lax.all_gather(dg, "fs", axis=0, tiled=True),
        lax.all_gather(dpt, "fs", axis=0, tiled=True),
    )
    full_v = jnp.dot(factor_value.astype(jnp.float32), whole_v, precision=lax.Precision.HIGHEST)
    full_g = jnp.dot(factor_gate.astype(jnp.float32), whole_g, precision=lax.Precision.HIGHEST)
    full_p = jnp.dot(factor_point.astype(jnp.float32), whole_p, precision=lax.Precision.HIGHEST)
    squares = lax.psum(
        (jnp.sum(full_v * full_v), jnp.sum(full_g * full_g), jnp.sum(full_p * full_p)), ("fs", "tp")
    )
    spread = lax.axis_size("fs") * lax.axis_size("tp")
    entries_in = full_v.shape[0] * full_v.shape[1] * spread
    entries_point = full_p.shape[0] * full_p.shape[1] * spread
    new_v = master_value - 0.1 * lax.rsqrt(squares[0] / entries_in + 1e-06) * full_v
    new_g = master_gate - 0.1 * lax.rsqrt(squares[1] / entries_in + 1e-06) * full_g
    new_p = master_point - 0.1 * lax.rsqrt(squares[2] / entries_point + 1e-06) * full_p
    copy_v, copy_g, copy_p = (
        lax.all_gather(new_v.astype(jnp.bfloat16), "fs", axis=0, tiled=True),
        lax.all_gather(new_g.astype(jnp.bfloat16), "fs", axis=0, tiled=True),
        lax.all_gather(new_p.astype(jnp.bfloat16), "fs", axis=0, tiled=True),
    )
    return (new_v, new_g, new_p, copy_v, copy_g, copy_p, fv, fg, fpt, sv, sg, spt)


def solution(mesh):
    return jax.shard_map(
        local,
        mesh=mesh,
        in_specs=(
            P("fs", None),
            P("fs", "tp"),
            P("fs", "tp"),
            P("fs", None),
            P("fs", "tp"),
            P("fs", "tp"),
            P("fs", "tp"),
            P("fs", "tp"),
            P("fs", None),
            P("fs", None),
            P("fs", None),
            P("fs", "tp"),
            P("fs", "tp"),
            P("fs", "tp"),
            P("fs", "tp"),
            P("fs", "tp"),
            P("fs", "tp"),
        ),
        out_specs=(
            P("fs", "tp"),
            P("fs", "tp"),
            P("fs", "tp"),
            P(None, "tp"),
            P(None, "tp"),
            P(None, "tp"),
            P("fs", "tp"),
            P("fs", "tp"),
            P("fs", "tp"),
            P("fs", "tp"),
            P("fs", "tp"),
            P("fs", "tp"),
        ),
        check_vma=False,
    )
```

profile of v0, /device:TPU:0, one launch (start us, length us, event | category | flops | bytes accessed | tf_op | source)
XLA Modules:
  0.0 531.6 jit_solution(17776841322710641022)
XLA Ops:
  7.2 33.4 %all_gather.31 = bf16[1024,256]{1,0:T(8,128)(2,1)S(1)} all-gather(bf16[128,256]{1,0:T(8,128)(2,1)} %param.27), channel_id=1, replica_groups=mesh['fs'=8,'tp'=4] {'fs'}, dimensions={0}, use_global_device_ids=true | all-gather | bytes 589824 | tf_op jit(solution)/shard_map/all_gather | solution.py:59
  40.6 3.5 fusion.14
  47.6 61.6 %reduce-scatter.8.cloned.1.call-done = f32[32,256]{1,0:T(8,128)} async-done(((f32[256,256]{1,0:T(8,128)}), f32[32,256]{1,0:T(8,128)}) %reduce-scatter.8.cloned.1.call-update) | async-done | bytes 32784 | tf_op jit(solution)/shard_map/reduce_scatter | solution.py:68
  109.2 1.4 add_divide_fusion
  110.6 31.4 %all_gather.32 = f32[256,256]{1,0:T(8,128)S(1)} all-gather(f32[32,256]{1,0:T(8,128)S(1)} %get-tuple-element.33), channel_id=1, replica_groups=mesh['fs'=8,'tp'=4] {'fs'}, dimensions={0}, use_global_device_ids=true | all-gather | bytes 294912 | tf_op jit(solution)/shard_map/all_gather | solution.py:76
  142.0 18.3 %all-gather.7.cloned.1.call-done = bf16[4096,256]{1,0:T(8,128)(2,1)} async-done(((bf16[512,256]{1,0:T(8,128)(2,1)}), bf16[4096,256]{1,0:T(8,128)(2,1)}) %all-gather.7.cloned.1.call-update) | async-done | bytes 2097168 | tf_op jit(solution)/shard_map/all_gather | solution.py:53
  160.3 8.7 %fusion.13 = f32[2048,256]{1,0:T(8,128)S(1)} fusion(bf16[2048,4096]{1,0:T(8,128)(2,1)} %param.17, bf16[4096,256]{1,0:T(8,128)(2,1)} %all-gather.7.cloned.1.call-done), kind=kOutput, calls=%fused_computation.34 | convolution fusion | flops 4294967296 | bytes 20971520 | tf_op jit(solution)/shard_map/dot_general | solution.py:51
  169.5 1.2 convolution_add_fusion.1
  170.8 39.5 %all-gather.5.cloned.1.call-done = bf16[4096,256]{1,0:T(8,128)(2,1)} async-done(((bf16[512,256]{1,0:T(8,128)(2,1)}), bf16[4096,256]{1,0:T(8,128)(2,1)}) %all-gather.5.cloned.1.call-update) | async-done | bytes 2097168 | tf_op jit(solution)/shard_map/all_gather | solution.py:48
  210.3 8.7 %fusion.12 = f32[2048,256]{1,0:T(8,128)S(1)} fusion(bf16[2048,4096]{1,0:T(8,128)(2,1)} %param.17, bf16[4096,256]{1,0:T(8,128)(2,1)} %all-gather.5.cloned.1.call-done), kind=kOutput, calls=%fused_computation.33 | convolution fusion | flops 4294967296 | bytes 20971520 | tf_op jit(solution)/shard_map/dot_general | solution.py:46
  219.6 1.2 convolution_add_fusion.2
  221.8 52.9 %reduce-scatter.6.cloned.1.call-done = f32[32,256]{1,0:T(8,128)} async-done(((f32[256,256]{1,0:T(8,128)}), f32[32,256]{1,0:T(8,128)}) %reduce-scatter.6.cloned.1.call-update) | async-done | bytes 32784 | tf_op jit(solution)/shard_map/reduce_scatter | solution.py:67
  274.7 1.4 add_divide_fusion.1
  276.1 30.9 %all_gather.30 = f32[256,256]{1,0:T(8,128)S(1)} all-gather(f32[32,256]{1,0:T(8,128)S(1)} %get-tuple-element.36), channel_id=1, replica_groups=mesh['fs'=8,'tp'=4] {'fs'}, dimensions={0}, use_global_device_ids=true | all-gather | bytes 294912 | tf_op jit(solution)/shard_map/all_gather | solution.py:75
  307.1 32.6 %reduce-scatter.4.cloned.1.call-done = f32[32,256]{1,0:T(8,128)} async-done(((f32[256,256]{1,0:T(8,128)}), f32[32,256]{1,0:T(8,128)}) %reduce-scatter.4.cloned.1.call-update) | async-done | bytes 32784 | tf_op jit(solution)/shard_map/reduce_scatter | solution.py:66
  339.6 1.4 add_divide_fusion.2
  341.0 30.8 %all_gather.28 = f32[256,256]{1,0:T(8,128)S(1)} all-gather(f32[32,256]{1,0:T(8,128)S(1)} %get-tuple-element.39), channel_id=1, replica_groups=mesh['fs'=8,'tp'=4] {'fs'}, dimensions={0}, use_global_device_ids=true | all-gather | bytes 294912 | tf_op jit(solution)/shard_map/all_gather | solution.py:74
  374.3 38.0 %all-reduce = (f32[]{:T(128)}, f32[]{:T(128)}, f32[]{:T(128)}) all-reduce(f32[]{:T(128)} %get-tuple-element.42, f32[]{:T(128)} %get-tuple-element.44, f32[]{:T(128)} %get-tuple-element.46), channel_id=1, replica_groups=mesh['fs'=8,'tp'=4] {'fs','tp'}, use_global_device_ids=true, to_apply=%region_2.0 | all-reduce | flops 3 | bytes 24 | tf_op jit(solution)/shard_map/psum | solution.py:81
  413.8 1.2 copy.30
  418.2 29.7 %all_gather.35 = bf16[1024,256]{0,1:T(8,128)(2,1)S(1)} all-gather(bf16[128,256]{0,1:T(8,128)(2,1)S(1)} %get-tuple-element.27), channel_id=1, replica_groups=mesh['fs'=8,'tp'=4] {'fs'}, dimensions={0}, use_global_device_ids=true | all-gather | bytes 589824 | tf_op jit(solution)/shard_map/all_gather | solution.py:93
  450.9 19.2 %all-gather.9.cloned.1.call-done = bf16[4096,256]{0,1:T(8,128)(2,1)} async-done(((bf16[512,256]{0,1:T(8,128)(2,1)}), bf16[4096,256]{0,1:T(8,128)(2,1)}) %all-gather.9.cloned.1.call-update) | async-done | bytes 2097168 | tf_op jit(solution)/shard_map/all_gather | solution.py:91
  470.1 4.1 copy.35
  474.2 46.5 %all-gather.11.cloned.1.call-done = bf16[4096,256]{0,1:T(8,128)(2,1)} async-done(((bf16[512,256]{0,1:T(8,128)(2,1)}), bf16[4096,256]{0,1:T(8,128)(2,1)}) %all-gather.11.cloned.1.call-update) | async-done | bytes 2097168 | tf_op jit(solution)/shard_map/all_gather | solution.py:92
  520.7 4.1 copy.36
  (58 shorter events, 13.6 us)
Async XLA Ops:
  7.2 36.9 %copy-start = (bf16[2048,256]{1,0:T(8,128)(2,1)S(1)}, bf16[2048,256]{1,0:T(8,128)(2,1)}, u32[]{:S(2)}) copy-start(bf16[2048,256]{1,0:T(8,128)(2,1)} %param.21) | copy-start | bytes 3145732
  7.2 102.0 %reduce-scatter.8.cloned.1.call-start = ((), (), s32[]{:S(2)}) async-start(), calls=%async_computation.7 | async-start | bytes 294912 | tf_op jit(solution)/shard_map/reduce_scatter | solution.py:68
  44.6 2.8 copy-start.5
  44.6 64.6 %copy-start.8 = (f32[32,256]{1,0:T(8,128)S(1)}, f32[32,256]{1,0:T(8,128)}, u32[]{:S(2)}) copy-start(f32[32,256]{1,0:T(8,128)} %param.33) | copy-start | bytes 98308
  44.6 64.6 %copy-start.9 = (f32[32,256]{1,0:T(8,128)S(1)}, f32[32,256]{1,0:T(8,128)}, u32[]{:S(2)}) copy-start(f32[32,256]{1,0:T(8,128)} %param.30) | copy-start | bytes 98308
  45.8 114.4 %all-gather.7.cloned.1.call-start = ((), (), s32[]{:S(2)}) async-start(), calls=%async_computation.5 | async-start | bytes 2359296 | tf_op jit(solution)/shard_map/all_gather | solution.py:53
  46.6 163.7 %all-gather.5.cloned.1.call-start = ((), (), s32[]{:S(2)}) async-start(), calls=%async_computation.3 | async-start | bytes 2359296 | tf_op jit(solution)/shard_map/all_gather | solution.py:48
  47.3 227.4 %reduce-scatter.6.cloned.1.call-start = ((), (), s32[]{:S(2)}) async-start(), calls=%async_computation.6 | async-start | bytes 294912 | tf_op jit(solution)/shard_map/reduce_scatter | solution.py:67
  142.0 27.0 %copy-start.1 = (bf16[2048,256]{1,0:T(8,128)(2,1)S(1)}, bf16[2048,256]{1,0:T(8,128)(2,1)}, u32[]{:S(2)}) copy-start(bf16[2048,256]{1,0:T(8,128)(2,1)} %param.19) | copy-start | bytes 3145732
  170.7 48.2 %copy-start.2 = (bf16[2048,256]{1,0:T(8,128)(2,1)S(1)}, bf16[2048,256]{1,0:T(8,128)(2,1)}, u32[]{:S(2)}) copy-start(bf16[2048,256]{1,0:T(8,128)(2,1)} %param.18) | copy-start | bytes 3145732
  170.7 168.9 %reduce-scatter.4.cloned.1.call-start = ((), (), s32[]{:S(2)}) async-start(), calls=%async_computation.4 | async-start | bytes 294912 | tf_op jit(solution)/shard_map/reduce_scatter | solution.py:66
  219.5 1.4 copy-start.6
  219.5 55.2 %copy-start.10 = (f32[32,256]{1,0:T(8,128)S(1)}, f32[32,256]{1,0:T(8,128)}, u32[]{:S(2)}) copy-start(f32[32,256]{1,0:T(8,128)} %param.32) | copy-start | bytes 98308
  219.5 55.2 %copy-start.11 = (f32[32,256]{1,0:T(8,128)S(1)}, f32[32,256]{1,0:T(8,128)}, u32[]{:S(2)}) copy-start(f32[32,256]{1,0:T(8,128)} %param.29) | copy-start | bytes 98308
  219.5 120.1 %copy-start.12 = (f32[32,256]{1,0:T(8,128)S(1)}, f32[32,256]{1,0:T(8,128)}, u32[]{:S(2)}) copy-start(f32[32,256]{1,0:T(8,128)} %param.31) | copy-start | bytes 98308
  219.5 120.1 %copy-start.13 = (f32[32,256]{1,0:T(8,128)S(1)}, f32[32,256]{1,0:T(8,128)}, u32[]{:S(2)}) copy-start(f32[32,256]{1,0:T(8,128)} %param.28) | copy-start | bytes 98308
  219.6 152.3 %copy-start.3 = (bf16[512,256]{1,0:T(8,128)(2,1)S(1)}, bf16[512,256]{1,0:T(8,128)(2,1)}, u32[]{:S(2)}) copy-start(bf16[512,256]{1,0:T(8,128)(2,1)} %param.25) | copy-start | bytes 786436
  220.8 152.3 %copy-start.4 = (bf16[512,256]{1,0:T(8,128)(2,1)S(1)}, bf16[512,256]{1,0:T(8,128)(2,1)}, u32[]{:S(2)}) copy-start(bf16[512,256]{1,0:T(8,128)(2,1)} %param.26) | copy-start | bytes 786436
  220.8 249.3 %all-gather.9.cloned.1.call-start = ((), (), s32[]{:S(2)}) async-start(), calls=%async_computation.8 | async-start | bytes 2359296 | tf_op jit(solution)/shard_map/all_gather | solution.py:91
  413.7 2.9 copy-start.7
  413.8 106.9 %all-gather.11.cloned.1.call-start = ((), (), s32[]{:S(2)}) async-start(), calls=%async_computation.9 | async-start | bytes 2359296 | tf_op jit(solution)/shard_map/all_gather | solution.py:92
Sparse Core Ops, SparseCore 0:
  46.0 63.1 reduce-scatter.7
  111.3 48.9 all-gather.6
  162.4 47.8 all-gather.4
  214.0 60.6 reduce-scatter.5
  278.5 61.1 reduce-scatter.3
  413.9 56.1 all-gather.8
  472.1 48.5 all-gather.10
where the time goes:
time: 532 us
  waiting for transfers between devices  272 us (51%)
  blocking collectives  194 us (36%)
  matrix products  29.3 us (6%)
  between operations  16.4 us (3%)
  local copies, waits for them, and re-layouts  13.5 us (3%)
  other arithmetic  5.86 us (1%)
    reduce_scatter x1, waiting for transfers between devices, local(): lax.psum_scatter(low_point, 'fs', scatter_dimension=0, tiled=True)  61.6 us
    reduce_scatter x1, waiting for transfers between devices, local(): lax.psum_scatter(low_gate, 'fs', scatter_dimension=0, tiled=True)  52.9 us
    all_gather x1, waiting for transfers between devices, local(): lax.all_gather(new_g.astype(jnp.bfloat16), 'fs', axis=0, tiled=True)  46.5 us
    all_gather x1, waiting for transfers between devices, local(): lax.all_gather(factor_value, 'fs', axis=0, tiled=True)  39.5 us
    psum x1, blocking collectives, local(): lax.psum((jnp.sum(full_v * full_v), jnp.sum(full_g * full_g), jnp.sum(ful...  38 us
    all_gather x1, blocking collectives, local(): lax.all_gather(factor_point, 'fs', axis=0, tiled=True)  33.4 us
    reduce_scatter x1, waiting for transfers between devices, local(): lax.psum_scatter(low_value, 'fs', scatter_dimension=0, tiled=True)  32.6 us
    all_gather x1, blocking collectives, local(): lax.all_gather(dpt, 'fs', axis=0, tiled=True)  31.4 us
  transfers between devices with their start and end apart: 7, of which 7 were waited for; matrix products, arithmetic and copies ran while one was open for 7% of the time, Pallas kernels for 0%

commit v1 on v0

--- a/solution.py
+++ b/solution.py
@@ -70,9 +70,32 @@
     fv, sv, dv = moments(summed[0] / total, first_value, second_value)
     fg, sg, dg = moments(summed[1] / total, first_gate, second_gate)
     fpt, spt, dpt = moments(summed[2] / total, first_point, second_point)
+
+    def _create_threads(state):
+        local_part = lax.axis_size("fs")
+        ready, block_now, reached = (local_part, lax.axis_index("fs"), state.shape[0])
+        line_up = [u * ready if kk == 0 else u for kk, u in enumerate(state.shape)]
+        part_next = lax.dynamic_update_slice_in_dim(
+            jnp.zeros(line_up, state.dtype), state, block_now * reached, axis=0
+        )
+        a_next = local_now = state
+        for c in range(1, ready // 2 + 1):
+            tile_out = list(map(lambda kk: (kk, (kk + 1) % ready), range(ready)))
+            a_next = lax.ppermute(a_next, "fs", tile_out)
+            part_next = lax.dynamic_update_slice_in_dim(
+                part_next, a_next, (block_now - c) % ready * reached, axis=0
+            )
+            if 2 * c < ready:
+                val2 = list(map(lambda kk: (kk, (kk - 1) % ready), range(ready)))
+                local_now = lax.ppermute(local_now, "fs", val2)
+                part_next = lax.dynamic_update_slice_in_dim(
+                    part_next, local_now, (block_now + c) % ready * reached, axis=0
+                )
+        return part_next
+
     whole_v, whole_g, whole_p = (
         lax.all_gather(dv, "fs", axis=0, tiled=True),
-        lax.all_gather(dg, "fs", axis=0, tiled=True),
+        _create_threads(dg),
         lax.all_gather(dpt, "fs", axis=0, tiled=True),
     )
     full_v = jnp.dot(factor_value.astype(jnp.float32), whole_v, precision=lax.Precision.HIGHEST)

time: 532 us -> 551 us (1.036)
  waiting for transfers between devices: 272 us -> 308 us
  blocking collectives: 194 us -> 163 us
  starting transfers between devices: 0.28 us -> 14.5 us
    all_gather x1 -> x0, blocking collectives: 30.9 us -> none  [local(): lax.all_gather(dg, 'fs', axis=0, tiled=True)]
    reduce_scatter x1, waiting for transfers between devices: 52.9 us -> 22 us  [local(): lax.psum_scatter(low_gate, 'fs', scatter_dimension=0, tiled=True)]
    all_gather x1, waiting for transfers between devices: 18.3 us -> 48.9 us  [local(): lax.all_gather(factor_gate, 'fs', axis=0, tiled=True)]
    reduce_scatter x1, waiting for transfers between devices: 32.6 us -> 58.8 us  [local(): lax.psum_scatter(low_value, 'fs', scatter_dimension=0, tiled=True)]
    ppermute x0 -> x7, starting transfers between devices: none -> 14.2 us  [the longest x3 12.7 us: _create_threads(): local_now = lax.ppermute(local_now, 'fs', val2)]
    ppermute x0 -> x7, waiting for transfers between devices: none -> 10.3 us  [the longest x4 10.3 us: _create_threads(): a_next = lax.ppermute(a_next, 'fs', tile_out)]
  transfers between devices with their start and end apart: 7 -> 14, of which waited for: 7 -> 10; matrix products, arithmetic and copies ran while one was open for 7% -> 7% of each run, Pallas kernels for 0% -> 0%
where the time goes in v1:
time: 551 us
  waiting for transfers between devices  308 us (56%)
  blocking collectives  163 us (30%)
  matrix products  29.3 us (5%)
  between operations  16.7 us (3%)
  starting transfers between devices  14.5 us (3%)
  local copies, waits for them, and re-layouts  13.5 us (2%)
  other arithmetic  5.85 us (1%)
    reduce_scatter x1, waiting for transfers between devices, local(): lax.psum_scatter(low_point, 'fs', scatter_dimension=0, tiled=True)  61.4 us
    reduce_scatter x1, waiting for transfers between devices, local(): lax.psum_scatter(low_value, 'fs', scatter_dimension=0, tiled=True)  58.8 us
    all_gather x1, waiting for transfers between devices, local(): lax.all_gather(factor_gate, 'fs', axis=0, tiled=True)  48.9 us
    all_gather x1, waiting for transfers between devices, local(): lax.all_gather(new_g.astype(jnp.bfloat16), 'fs', axis=0, tiled=True)  46.5 us
    all_gather x1, waiting for transfers between devices, local(): lax.all_gather(factor_value, 'fs', axis=0, tiled=True)  39.3 us
    psum x1, blocking collectives, local(): lax.psum((jnp.sum(full_v * full_v), jnp.sum(full_g * full_g), jnp.sum(ful...  37.3 us
    all_gather x1, blocking collectives, local(): lax.all_gather(factor_point, 'fs', axis=0, tiled=True)  33.4 us
    all_gather x1, blocking collectives, local(): lax.all_gather(dv, 'fs', axis=0, tiled=True)  31 us
  transfers between devices with their start and end apart: 14, of which 10 were waited for; matrix products, arithmetic and copies ran while one was open for 7% of the time, Pallas kernels for 0%

profile of v1, /device:TPU:0, one launch (start us, length us, event | category | flops | bytes accessed | tf_op | source)
XLA Modules:
  0.0 550.7 jit_solution(12630729554457841299)
XLA Ops:
  7.2 33.4 %all_gather.27 = bf16[1024,256]{1,0:T(8,128)(2,1)S(1)} all-gather(bf16[128,256]{1,0:T(8,128)(2,1)} %param.27), channel_id=1, replica_groups=mesh['fs'=8,'tp'=4] {'fs'}, dimensions={0}, use_global_device_ids=true | all-gather | bytes 589824 | tf_op jit(solution)/shard_map/all_gather | solution.py:59
  40.6 3.5 fusion.14
  47.8 61.4 %reduce-scatter.8.cloned.1.call-done = f32[32,256]{1,0:T(8,128)} async-done(((f32[256,256]{1,0:T(8,128)}), f32[32,256]{1,0:T(8,128)}) %reduce-scatter.8.cloned.1.call-update) | async-done | bytes 32784 | tf_op jit(solution)/shard_map/reduce_scatter | solution.py:68
  110.6 48.9 %all-gather.7.cloned.1.call-done = bf16[4096,256]{1,0:T(8,128)(2,1)} async-done(((bf16[512,256]{1,0:T(8,128)(2,1)}), bf16[4096,256]{1,0:T(8,128)(2,1)}) %all-gather.7.cloned.1.call-update) | async-done | bytes 2097168 | tf_op jit(solution)/shard_map/all_gather | solution.py:53
  159.5 8.7 %fusion.13 = f32[2048,256]{1,0:T(8,128)S(1)} fusion(bf16[2048,4096]{1,0:T(8,128)(2,1)} %param.17, bf16[4096,256]{1,0:T(8,128)(2,1)} %all-gather.7.cloned.1.call-done), kind=kOutput, calls=%fused_computation.42 | convolution fusion | flops 4294967296 | bytes 20971520 | tf_op jit(solution)/shard_map/dot_general | solution.py:51
  170.0 39.3 %all-gather.5.cloned.1.call-done = bf16[4096,256]{1,0:T(8,128)(2,1)} async-done(((bf16[512,256]{1,0:T(8,128)(2,1)}), bf16[4096,256]{1,0:T(8,128)(2,1)}) %all-gather.5.cloned.1.call-update) | async-done | bytes 2097168 | tf_op jit(solution)/shard_map/all_gather | solution.py:48
  209.3 8.7 %fusion.12 = f32[2048,256]{1,0:T(8,128)S(1)} fusion(bf16[2048,4096]{1,0:T(8,128)(2,1)} %param.17, bf16[4096,256]{1,0:T(8,128)(2,1)} %all-gather.5.cloned.1.call-done), kind=kOutput, calls=%fused_computation.41 | convolution fusion | flops 4294967296 | bytes 20971520 | tf_op jit(solution)/shard_map/dot_general | solution.py:46
  219.8 30.9 %all_gather.28 = f32[256,256]{1,0:T(8,128)S(1)} all-gather(f32[32,256]{1,0:T(8,128)S(1)} %get-tuple-element.33), channel_id=1, replica_groups=mesh['fs'=8,'tp'=4] {'fs'}, dimensions={0}, use_global_device_ids=true | all-gather | bytes 294912 | tf_op jit(solution)/shard_map/all_gather | solution.py:99
  251.7 22.0 %reduce-scatter.6.cloned.1.call-done = f32[32,256]{1,0:T(8,128)} async-done(((f32[256,256]{1,0:T(8,128)}), f32[32,256]{1,0:T(8,128)}) %reduce-scatter.6.cloned.1.call-update) | async-done | bytes 32784 | tf_op jit(solution)/shard_map/reduce_scatter | solution.py:67
  275.1 1.4 collective-permute-start
  276.6 3.3 collective-permute-start.1
  279.9 58.8 %reduce-scatter.4.cloned.1.call-done = f32[32,256]{1,0:T(8,128)} async-done(((f32[256,256]{1,0:T(8,128)}), f32[32,256]{1,0:T(8,128)}) %reduce-scatter.4.cloned.1.call-update) | async-done | bytes 32784 | tf_op jit(solution)/shard_map/reduce_scatter | solution.py:66
  340.0 31.0 %all_gather.25 = f32[256,256]{1,0:T(8,128)S(1)} all-gather(f32[32,256]{1,0:T(8,128)S(1)} %get-tuple-element.40), channel_id=1, replica_groups=mesh['fs'=8,'tp'=4] {'fs'}, dimensions={0}, use_global_device_ids=true | all-gather | bytes 294912 | tf_op jit(solution)/shard_map/all_gather | solution.py:97
  372.2 4.7 collective-permute-start.3
  377.0 1.9 collective-permute-done.2
  378.9 4.7 collective-permute-start.5
  383.6 1.9 collective-permute-done.4
  385.5 6.6 %collective-permute-done.6 = f32[32,256]{1,0:T(8,128)S(1)} collective-permute-done((f32[32,256]{1,0:T(8,128)S(1)}, f32[32,256]{1,0:T(8,128)S(1)}, u32[]{:S(2)}, u32[]{:S(2)}) %collective-permute-start.6) | collective-permute-done | bytes 32800 | tf_op jit(solution)/shard_map/ppermute | solution.py:84
  393.3 37.3 %all-reduce = (f32[]{:T(128)}, f32[]{:T(128)}, f32[]{:T(128)}) all-reduce(f32[]{:T(128)} %get-tuple-element.43, f32[]{:T(128)} %get-tuple-element.45, f32[]{:T(128)} %get-tuple-element.47), channel_id=1, replica_groups=mesh['fs'=8,'tp'=4] {'fs','tp'}, use_global_device_ids=true, to_apply=%region_2.0 | all-reduce | flops 3 | bytes 24 | tf_op jit(solution)/shard_map/psum | solution.py:104
  436.6 30.0 %all_gather.31 = bf16[1024,256]{0,1:T(8,128)(2,1)S(1)} all-gather(bf16[128,256]{0,1:T(8,128)(2,1)S(1)} %get-tuple-element.27), channel_id=1, replica_groups=mesh['fs'=8,'tp'=4] {'fs'}, dimensions={0}, use_global_device_ids=true | all-gather | bytes 589824 | tf_op jit(solution)/shard_map/all_gather | solution.py:116
  469.5 19.7 %all-gather.9.cloned.1.call-done = bf16[4096,256]{0,1:T(8,128)(2,1)} async-done(((bf16[512,256]{0,1:T(8,128)(2,1)}), bf16[4096,256]{0,1:T(8,128)(2,1)}) %all-gather.9.cloned.1.call-update) | async-done | bytes 2097168 | tf_op jit(solution)/shard_map/all_gather | solution.py:114
  489.2 4.1 copy.35
  493.3 46.5 %all-gather.11.cloned.1.call-done = bf16[4096,256]{0,1:T(8,128)(2,1)} async-done(((bf16[512,256]{0,1:T(8,128)(2,1)}), bf16[4096,256]{0,1:T(8,128)(2,1)}) %all-gather.11.cloned.1.call-update) | async-done | bytes 2097168 | tf_op jit(solution)/shard_map/all_gather | solution.py:115
  539.8 4.1 copy.36
  (79 shorter events, 21.5 us)
Async XLA Ops:
  7.2 102.0 %reduce-scatter.8.cloned.1.call-start = ((), (), s32[]{:S(2)}) async-start(), calls=%async_computation.7 | async-start | bytes 294912 | tf_op jit(solution)/shard_map/reduce_scatter | solution.py:68
  44.6 64.6 %copy-start.10 = (f32[32,256]{1,0:T(8,128)S(1)}, f32[32,256]{1,0:T(8,128)}, u32[]{:S(2)}) copy-start(f32[32,256]{1,0:T(8,128)} %param.33) | copy-start | bytes 98308
  44.6 64.6 %copy-start.11 = (f32[32,256]{1,0:T(8,128)S(1)}, f32[32,256]{1,0:T(8,128)}, u32[]{:S(2)}) copy-start(f32[32,256]{1,0:T(8,128)} %param.30) | copy-start | bytes 98308
  45.9 113.6 %all-gather.7.cloned.1.call-start = ((), (), s32[]{:S(2)}) async-start(), calls=%async_computation.5 | async-start | bytes 2359296 | tf_op jit(solution)/shard_map/all_gather | solution.py:53
  46.6 162.6 %all-gather.5.cloned.1.call-start = ((), (), s32[]{:S(2)}) async-start(), calls=%async_computation.3 | async-start | bytes 2359296 | tf_op jit(solution)/shard_map/all_gather | solution.py:48
  47.3 226.4 %reduce-scatter.6.cloned.1.call-start = ((), (), s32[]{:S(2)}) async-start(), calls=%async_computation.6 | async-start | bytes 294912 | tf_op jit(solution)/shard_map/reduce_scatter | solution.py:67
  110.6 57.6 %copy-start.1 = (bf16[2048,256]{1,0:T(8,128)(2,1)S(1)}, bf16[2048,256]{1,0:T(8,128)(2,1)}, u32[]{:S(2)}) copy-start(bf16[2048,256]{1,0:T(8,128)(2,1)} %param.19) | copy-start | bytes 3145732
  169.9 48.1 %copy-start.2 = (bf16[2048,256]{1,0:T(8,128)(2,1)S(1)}, bf16[2048,256]{1,0:T(8,128)(2,1)}, u32[]{:S(2)}) copy-start(bf16[2048,256]{1,0:T(8,128)(2,1)} %param.18) | copy-start | bytes 3145732
  169.9 168.7 %reduce-scatter.4.cloned.1.call-start = ((), (), s32[]{:S(2)}) async-start(), calls=%async_computation.4 | async-start | bytes 294912 | tf_op jit(solution)/shard_map/reduce_scatter | solution.py:66
  218.5 55.2 %copy-start.8 = (f32[32,256]{1,0:T(8,128)S(1)}, f32[32,256]{1,0:T(8,128)}, u32[]{:S(2)}) copy-start(f32[32,256]{1,0:T(8,128)} %param.32) | copy-start | bytes 98308
  218.5 55.2 %copy-start.9 = (f32[32,256]{1,0:T(8,128)S(1)}, f32[32,256]{1,0:T(8,128)}, u32[]{:S(2)}) copy-start(f32[32,256]{1,0:T(8,128)} %param.29) | copy-start | bytes 98308
  218.5 120.1 %copy-start.12 = (f32[32,256]{1,0:T(8,128)S(1)}, f32[32,256]{1,0:T(8,128)}, u32[]{:S(2)}) copy-start(f32[32,256]{1,0:T(8,128)} %param.31) | copy-start | bytes 98308
  218.5 120.1 %copy-start.13 = (f32[32,256]{1,0:T(8,128)S(1)}, f32[32,256]{1,0:T(8,128)}, u32[]{:S(2)}) copy-start(f32[32,256]{1,0:T(8,128)} %param.28) | copy-start | bytes 98308
  218.5 152.5 %copy-start.3 = (bf16[512,256]{1,0:T(8,128)(2,1)S(1)}, bf16[512,256]{1,0:T(8,128)(2,1)}, u32[]{:S(2)}) copy-start(bf16[512,256]{1,0:T(8,128)(2,1)} %param.25) | copy-start | bytes 786436
  219.8 172.3 %copy-start.4 = (bf16[512,256]{1,0:T(8,128)(2,1)S(1)}, bf16[512,256]{1,0:T(8,128)(2,1)}, u32[]{:S(2)}) copy-start(bf16[512,256]{1,0:T(8,128)(2,1)} %param.26) | copy-start | bytes 786436
  219.8 269.4 %all-gather.9.cloned.1.call-start = ((), (), s32[]{:S(2)}) async-start(), calls=%async_computation.8 | async-start | bytes 2359296 | tf_op jit(solution)/shard_map/all_gather | solution.py:114
  275.1 97.1 %collective-permute-start = (f32[32,256]{1,0:T(8,128)S(1)}, f32[32,256]{1,0:T(8,128)S(1)}, u32[]{:S(2)}, u32[]{:S(2)}) collective-permute-start(f32[32,256]{1,0:T(8,128)S(1)} %get-tuple-element.37), channel_id=1, source_target_pairs={{0,4},{4,8},{8,12},{12,16},{16,20},{20,24},{24,28},{28,0},{1,5},{5... | collective-permute-start | bytes 98312 | tf_op jit(solution)/shard_map/ppermute | solution.py:84
  276.6 95.7 %collective-permute-start.1 = (f32[32,256]{1,0:T(8,128)S(1)}, f32[32,256]{1,0:T(8,128)S(1)}, u32[]{:S(2)}, u32[]{:S(2)}) collective-permute-start(f32[32,256]{1,0:T(8,128)S(1)} %get-tuple-element.37), channel_id=1, source_target_pairs={{0,28},{4,0},{8,4},{12,8},{16,12},{20,16},{24,20},{28,24},{1,29},{... | collective-permute-start | bytes 98312 | tf_op jit(solution)/shard_map/ppermute | solution.py:90
  372.2 6.6 %collective-permute-start.2 = (f32[32,256]{1,0:T(8,128)S(1)}, f32[32,256]{1,0:T(8,128)S(1)}, u32[]{:S(2)}, u32[]{:S(2)}) collective-permute-start(f32[32,256]{1,0:T(8,128)S(1)} %collective-permute-done), channel_id=1, source_target_pairs={{0,4},{4,8},{8,12},{12,16},{16,20},{20,24},{24,28},{28,0},{1,5},{5... | collective-permute-start | bytes 98312 | tf_op jit(solution)/shard_map/ppermute | solution.py:84
  372.2 6.6 %collective-permute-start.3 = (f32[32,256]{1,0:T(8,128)S(1)}, f32[32,256]{1,0:T(8,128)S(1)}, u32[]{:S(2)}, u32[]{:S(2)}) collective-permute-start(f32[32,256]{1,0:T(8,128)S(1)} %collective-permute-done.1), channel_id=1, source_target_pairs={{0,28},{4,0},{8,4},{12,8},{16,12},{20,16},{24,20},{28,24},{1,29},{... | collective-permute-start | bytes 98312 | tf_op jit(solution)/shard_map/ppermute | solution.py:90
  378.9 6.6 %collective-permute-start.4 = (f32[32,256]{1,0:T(8,128)S(1)}, f32[32,256]{1,0:T(8,128)S(1)}, u32[]{:S(2)}, u32[]{:S(2)}) collective-permute-start(f32[32,256]{1,0:T(8,128)S(1)} %collective-permute-done.2), channel_id=1, source_target_pairs={{0,4},{4,8},{8,12},{12,16},{16,20},{20,24},{24,28},{28,0},{1,5},{5... | collective-permute-start | bytes 98312 | tf_op jit(solution)/shard_map/ppermute | solution.py:84
  378.9 6.6 %collective-permute-start.5 = (f32[32,256]{1,0:T(8,128)S(1)}, f32[32,256]{1,0:T(8,128)S(1)}, u32[]{:S(2)}, u32[]{:S(2)}) collective-permute-start(f32[32,256]{1,0:T(8,128)S(1)} %collective-permute-done.3), channel_id=1, source_target_pairs={{0,28},{4,0},{8,4},{12,8},{16,12},{20,16},{24,20},{28,24},{1,29},{... | collective-permute-start | bytes 98312 | tf_op jit(solution)/shard_map/ppermute | solution.py:90
  385.5 6.6 %collective-permute-start.6 = (f32[32,256]{1,0:T(8,128)S(1)}, f32[32,256]{1,0:T(8,128)S(1)}, u32[]{:S(2)}, u32[]{:S(2)}) collective-permute-start(f32[32,256]{1,0:T(8,128)S(1)} %collective-permute-done.4), channel_id=1, source_target_pairs={{0,4},{4,8},{8,12},{12,16},{16,20},{20,24},{24,28},{28,0},{1,5},{5... | collective-permute-start | bytes 98312 | tf_op jit(solution)/shard_map/ppermute | solution.py:84
  432.1 107.7 %all-gather.11.cloned.1.call-start = ((), (), s32[]{:S(2)}) async-start(), calls=%async_computation.9 | async-start | bytes 2359296 | tf_op jit(solution)/shard_map/all_gather | solution.py:115
  (4 other events, 74.9 us)
Sparse Core Ops, SparseCore 0:
  46.0 63.1 reduce-scatter.7
  111.3 48.1 all-gather.6
  161.6 47.6 all-gather.4
  213.0 60.6 reduce-scatter.5
  277.4 61.1 reduce-scatter.3
  432.3 56.9 all-gather.8
  491.3 48.5 all-gather.10
